TPU v7x, 1024 devices: a whole 4x4x32 slice. The times are simulated.
1024 devices in a mesh: sp: 128 (over z, y), tp: 8 (over x, core).
Axes of the slice: x: 4, y: 4, z: 32, core: 2. Of those that a mesh axis runs over, the one named last changes fastest.
Arguments:
- tokens: bfloat16 [2, 8192, 4096], P(None, 'sp'), may hold values from -28 to 28
- w_forget: bfloat16 [4096, 2048], P(None, 'tp'), may hold values from -0.09375 to 0.09375
- w_value: bfloat16 [4096, 2048], P(None, 'tp'), may hold values from -0.375 to 0.375
- floor_logit: float32 [2048], P('tp'), may hold values from 0.5 to 11.5
- norm_gain: float32 [128], replicated, may hold values from 0.1 to 1.9
- query_new: bfloat16 [2, 2048], P(None, 'tp'), may hold values from -6 to 6
- gate_new: bfloat16 [2, 2048], P(None, 'tp'), may hold values from -6 to 6
- w_out: bfloat16 [2048, 4096], P('tp'), may hold values from -0.125 to 0.125
Outputs:
- state_cache: bfloat16 [2, 16, 128, 128], P(None, 'tp', 'sp')
- decode_out: bfloat16 [2, 4096], P(None, 'tp')
All inputs are finite; a program needn't handle non-finite values.
Results may differ from a plain program's by a relative error of at most 0.014.
Values may be sent and summed in bfloat16 or wider, within the bound.
A program may use at most 64 MiB of HBM per device.

v0:
```python
import functools

import jax
import jax.numpy as jnp
from jax import lax
from jax.sharding import Mesh
from jax.sharding import PartitionSpec as P

DK = 128
SP = ("sp_0", "sp_1")


epsilon = 1e-06


def prefix(value, axis, join, neutral):
    count, mine = (lax.axis_size(axis), lax.axis_index(axis))
    pieces = lax.all_gather(value, axis)
    pieces = pieces[::-1]
    mine = count - 1 - mine
    running = jnp.full_like(value, 0) + jnp.asarray(neutral, value.dtype)

    def hop(position, running):
        longer = join(running, pieces[position])
        return jnp.where(position < mine, longer, running)

    return lax.fori_loop(0, count - 1, hop, running)


def sum_by_axis(x, axes, dim):
    if not axes:
        return x
    nearer = lax.psum_scatter(x, axes[0], scatter_dimension=dim, tiled=True)
    return sum_by_axis(nearer, axes[1:], dim)


def over_axes(x, axes):
    return functools.reduce(lax.psum, axes, x)


def cut_along(x, dim, count):
    lengths = x.shape
    tiles = x.reshape(*lengths[:dim], count, lengths[dim] // count, *lengths[dim + 1 :])
    return jnp.moveaxis(tiles, dim, 0)


def sent_and_summed(x, axis, dim):
    tiles = cut_along(x, dim, lax.axis_size(axis))
    arrived = lax.all_to_all(tiles, axis, split_axis=0, concat_axis=0, tiled=True)
    return arrived.astype(jnp.float32).sum(axis=0)


def forget_terms(forget_pre, floor_heads):
    forget_f32 = forget_pre.astype(jnp.float32)
    log_keep = jnp.logaddexp(
        jax.nn.log_sigmoid(floor_heads),
        jax.nn.log_sigmoid(-floor_heads) + jax.nn.log_sigmoid(forget_f32),
    )
    key_gate = jax.nn.sigmoid(-floor_heads) * jax.nn.sigmoid(-forget_f32)
    return (log_keep, key_gate)


def span_state(block_tokens, w_forget, w_value, floor_heads):
    num_seqs, span_len, model_width = block_tokens.shape
    flat = block_tokens.reshape(num_seqs * span_len, model_width)
    forget_pre = jnp.dot(flat, w_forget, preferred_element_type=jnp.float32).astype(jnp.bfloat16)
    values = jnp.dot(flat, w_value, preferred_element_type=jnp.float32).astype(jnp.bfloat16)
    forget_pre = forget_pre.reshape(num_seqs, span_len, floor_heads.shape[0], floor_heads.shape[1])
    values = values.reshape(num_seqs, span_len, floor_heads.shape[0], -1)
    log_keep, key_gate = forget_terms(forget_pre, floor_heads)
    running = jnp.cumsum(log_keep, axis=1)
    block_total = running[:, -1]
    weighted = key_gate * jnp.exp(block_total[:, None] - running)
    own_state = jnp.einsum("nshk,nshv->nhkv", weighted, values.astype(jnp.float32))
    return (block_total, own_state)


def gated_read(read_raw, norm_gain, gate_new):
    scale = lax.rsqrt(jnp.mean(read_raw * read_raw, axis=-1, keepdims=True) + epsilon)
    normed = read_raw * scale * norm_gain
    normed = normed.reshape(normed.shape[0], -1)
    return (normed * jax.nn.silu(gate_new.astype(jnp.float32))).astype(jnp.bfloat16)


def add_totals(early, late):
    return early + late


def on_device(tokens, w_forget, w_value, floor_logit, norm_gain, query_new, gate_new, w_out):
    local_heads = w_forget.shape[1] // DK
    floor_heads = floor_logit.reshape(local_heads, DK)
    block_total, own_state = span_state(tokens, w_forget, w_value, floor_heads)
    num_seqs = tokens.shape[0]
    query = jax.nn.silu(query_new.astype(jnp.float32)).reshape(num_seqs, local_heads, DK)
    row_count = DK // lax.axis_size(SP)
    row_start = lax.axis_index(SP) * row_count
    decay_after = prefix(block_total, SP, add_totals, jnp.zeros_like(block_total))
    contrib = jnp.exp(decay_after)[..., None] * own_state
    my_rows = sum_by_axis(contrib, SP, 2)
    state_cache = my_rows.astype(jnp.bfloat16)
    query_rows = lax.dynamic_slice_in_dim(query, row_start, row_count, 2)
    partial_read = jnp.einsum("nhk,nhkv->nhv", query_rows, my_rows)
    read_raw = over_axes(partial_read, SP)
    read = gated_read(read_raw, norm_gain, gate_new)
    out_term = jnp.dot(read, w_out, preferred_element_type=jnp.float32)
    decode_out = sent_and_summed(out_term.astype(jnp.bfloat16), "tp", 1).astype(jnp.bfloat16)
    return (state_cache, decode_out)


def solution(mesh):
    torus = Mesh(mesh.devices.reshape(32, 4, mesh.shape["tp"]), ("sp_0", "sp_1", "tp"))
    return jax.shard_map(
        on_device,
        mesh=torus,
        in_specs=(
            P(None, SP, None),
            P(None, "tp"),
            P(None, "tp"),
            P("tp"),
            P(),
            P(None, "tp"),
            P(None, "tp"),
            P("tp", None),
        ),
        out_specs=(P(None, "tp", SP, None), P(None, "tp")),
        check_vma=False,
    )
```

profile of v0, /device:TPU:1, one launch (start us, length us, event | category | flops | bytes accessed | tf_op | source)
XLA Modules:
  0.0 670.8 jit_solution(15148756973285256924)
XLA Ops:
  7.2 1.5 copy-done
  8.8 1.8 add_divide_fusion
  10.6 0.7 fusion.35
  12.0 0.7 div.25
  12.7 162.4 %all-gather = f32[256,1,2,128]{3,2,1,0:T(2,128)S(1)} all-gather(f32[2,1,2,128]{3,2,1,0:T(2,128)S(1)} %get-tuple-element.109), channel_id=2, replica_groups=mesh['sp_0'=32,'sp_1'=4,'tp'=8] {'sp_0','sp_1'}, dimensions={0}, use_global_device_ids=true | all-gather | bytes 264192 | tf_op jit(solution)/shard_map/all_gather | solution.py:18
  175.2 0.7 rev.3
  175.9 86.6 %while.14 = (s32[]{:T(128)}, f32[2,2,128]{2,1,0:T(2,128)S(1)}, s32[]{:T(128)}, f32[128,2,2,128]{3,2,1,0:T(2,128)}, s32[]{:T(128)}, /*index=5*/s32[]{:T(128)}) while((s32[]{:T(128)}, f32[2,2,128]{2,1,0:T(2,128)S(1)}, s32[]{:T(128)}, f32[128,2,2,128]{3,2,1,0:T(2,128)}, s32[]{:T(128)}, /*index=5*/s32[]{:T(128)}) %tuple.44), condition=%wide.region_2.3_spmd.clone, body=%wide.region_1.2_spmd.clone.sunk | while | flops 1540 | bytes 6237 | solution.py:27
  175.9 0.7 add_select_fusion.2
  184.8 0.7 add_select_fusion.2
  189.5 0.7 add_select_fusion.2
  205.2 0.7 add_select_fusion.2
  225.0 0.7 add_select_fusion.2
  238.6 0.7 add_select_fusion.2
  240.0 0.7 add_select_fusion.2
  245.5 0.7 add_select_fusion.2
  253.6 0.7 add_select_fusion.2
  260.5 0.7 add_select_fusion.2
  262.5 2.0 convolution_convert_fusion.1
  264.7 0.9 convolution_multiply_fusion
  266.6 1.3 dynamic-slice
  267.9 1.3 dynamic-slice.2
  269.8 286.3 %all-reduce.4.cloned.1.call-done = f32[2,2,128,128]{3,2,1,0:T(8,128)} async-done(((f32[2,2,128,128]{3,2,1,0:T(8,128)}), f32[2,2,128,128]{3,2,1,0:T(8,128)}) %all-reduce.4.cloned.1.call-update) | async-done | bytes 262160
  556.1 0.7 constant_dynamic-slice_fusion
  556.8 8.8 %all-reduce.1 = f32[2,2,4,128]{3,1,0,2:T(2,128)S(1)} all-reduce(f32[2,2,4,128]{3,1,0,2:T(2,128)S(1)} %copy.16), channel_id=4, replica_groups=mesh['sp_0'=32,'sp_1'=4,'tp'=8] {'sp_1'}, use_global_device_ids=true, to_apply=%region_4.5.clone | all-reduce | flops 2048 | bytes 16384
  565.6 0.7 bitcast_multiply_fusion
  566.3 40.7 %psum.14 = f32[2,2,128]{2,1,0:T(2,128)S(1)} all-reduce(f32[2,2,128]{2,1,0:T(2,128)S(1)} %bitcast_multiply_fusion), channel_id=1, replica_groups=mesh['sp_0'=32,'sp_1'=4,'tp'=8] {'sp_0'}, use_global_device_ids=true, to_apply=%region_5.6 | all-reduce | flops 512 | bytes 4096 | tf_op jit(solution)/shard_map/psum | solution.py:38
  607.1 6.1 psum.15
  613.3 0.7 multiply_bitcast_fusion
  614.0 2.6 convolution_convert_fusion
  616.6 42.1 %all-to-all-start = ((bf16[8,2,512]{2,1,0:T(2,128)(2,1)}), bf16[8,2,512]{2,1,0:T(2,128)(2,1)S(1)}, u32[]{:S(2)}, u32[]{:S(2)}) async-start(bf16[8,2,512]{2,1,0:T(2,128)(2,1)} %bitcast.8), calls=%async_computation | async-start | bytes 32768 | tf_op jit(solution)/shard_map/all_to_all | solution.py:49
  658.7 1.2 fusion.31
  659.9 3.4 all-to-all-done
  (141 shorter events, 82.1 us)
Async XLA Ops:
  7.2 1.6 copy-start
  7.2 548.9 %all-reduce.4.cloned.1.call-start = ((), (), s32[]{:S(2)}) async-start(), calls=%async_computation.1 | async-start | bytes 524288
  8.8 253.8 %copy-start.1 = (bf16[2,64,4096]{2,1,0:T(8,128)(2,1)S(1)}, bf16[2,64,4096]{2,1,0:T(8,128)(2,1)}, u32[]{:S(2)}) copy-start(bf16[2,64,4096]{2,1,0:T(8,128)(2,1)} %param.10) | copy-start | bytes 3145732
  175.9 88.7 %copy-start.2 = (f32[2,64,2,128]{3,2,1,0:T(2,128)S(1)}, f32[2,64,2,128]{3,2,1,0:T(2,128)}, u32[]{:S(2)}) copy-start(f32[2,64,2,128]{3,2,1,0:T(2,128)} %div.25) | copy-start | bytes 393220
  262.5 351.5 %copy-start.3 = (bf16[2,256]{1,0:T(2,128)(2,1)S(1)}, bf16[2,256]{1,0:T(2,128)(2,1)}, u32[]{:S(2)}) copy-start(bf16[2,256]{1,0:T(2,128)(2,1)} %param.16) | copy-start | bytes 3076
  616.6 46.7 %all-to-all-start = ((bf16[8,2,512]{2,1,0:T(2,128)(2,1)}), bf16[8,2,512]{2,1,0:T(2,128)(2,1)S(1)}, u32[]{:S(2)}, u32[]{:S(2)}) async-start(bf16[8,2,512]{2,1,0:T(2,128)(2,1)} %bitcast.8), calls=%async_computation | async-start | bytes 32768 | tf_op jit(solution)/shard_map/all_to_all | solution.py:49
Sparse Core Ops, SparseCore 0:
  265.8 290.2 all-reduce.3
where the time goes:
time: 674 us; the launch traced here: 671 us
  waiting for transfers between devices  290 us (43%)
  blocking collectives  218 us (32%)
  other arithmetic  90.9 us (13%)
  starting transfers between devices  42.1 us (6%)
  between operations  14.8 us (2%)
  local copies, waits for them, and re-layouts  7.79 us (1%)
  matrix products  7.32 us (1%)
    unnamed x2, waiting for transfers between devices  286 us
    all_gather x1, blocking collectives, prefix(): pieces = lax.all_gather(value, axis)  162 us
    select_n x127, other arithmetic, hop(): return jnp.where(position < mine, longer, running)  86.5 us
    psum x2, blocking collectives, over_axes(): return functools.reduce(lax.psum, axes, x)  46.8 us
    all_to_all x1, starting transfers between devices, sent_and_summed(): lax.all_to_all(tiles, axis, split_axis=0, concat_axis=0, tiled=True)  42.1 us
  transfers between devices with their start and end apart: 2, of which 2 were waited for; matrix products, arithmetic and copies ran while one was open for 1% of the time, Pallas kernels for 0%

commit v1 on v0

v1 whole, which is shorter than its diff:
```python
import functools

import jax
import jax.numpy as jnp
from jax import lax
from jax.experimental import pallas as pl
from jax.experimental.pallas import tpu as pltpu
from jax.sharding import PartitionSpec as P

MESH = pl.DeviceIdType.MESH
F32 = jnp.float32
BF16 = jnp.bfloat16
EPSILON = 1e-06

DK = 128
PLANE = 16
GROUPS = 8
ROWS = 32
N_TP = 8
CHUNKS = 4
SENDS = (4, 3, 5, 2, 6, 1, 7)


def kernel(
    tok, w_forget, w_value, floor, gain, query, gate, w_out,
    state_out, decode_out,
    tok_v, wf_v, wv_v, wo_v, floor_v, gain_v, query_v, gate_v,
    send1, total1, recv1, rtotal1,
    send3, total3, recv3, rtotal3,
    part4, recv4, row4, rrow4, send5, recv5,
    in_sem, small_sem, wo_sem,
    s1, r1, st1, rt1, s3, r3, st3, rt3, s4, r4, sr4, rr4, s5, r5,
):
    sp, tp = lax.axis_index("sp"), lax.axis_index("tp")
    group, me = sp // PLANE, sp % PLANE
    slice_m, pair = me // 4, me % 4
    depth = tok.shape[1] // CHUNKS

    loads = []
    for c in range(CHUNKS):
        ks = pl.ds(c * depth, depth)
        loads.append([
            pltpu.make_async_copy(tok.at[:, ks], tok_v.at[:, ks], in_sem.at[3 * c]),
            pltpu.make_async_copy(w_forget.at[ks], wf_v.at[ks], in_sem.at[3 * c + 1]),
            pltpu.make_async_copy(w_value.at[ks], wv_v.at[ks], in_sem.at[3 * c + 2]),
        ])
    smalls = [
        pltpu.make_async_copy(src, dst, small_sem.at[i])
        for i, (src, dst) in enumerate(((floor, floor_v), (gain, gain_v), (query, query_v), (gate, gate_v)))
    ]
    load_out = pltpu.make_async_copy(w_out, wo_v, wo_sem)
    for copy in loads[0]:
        copy.start()
    for copy in smalls:
        copy.start()
    for chunk in loads[1:]:
        for copy in chunk:
            copy.start()
    load_out.start()

    barrier = pltpu.get_barrier_semaphore()

    def in_plane(j):
        other = (me + j) % PLANE
        return other, (group * PLANE + other, tp)

    def in_line(j):
        other = (group + j) % GROUPS
        return other, (other * PLANE + me, tp)

    def in_tp(j):
        other = (tp + j) % N_TP
        return other, (sp, other)

    partners = [in_line(j)[1] for j in SENDS]
    partners += [in_plane(j)[1] for j in range(1, PLANE)]
    partners += [in_tp(j)[1] for j in range(1, N_TP)]
    for device in partners:
        pl.semaphore_signal(barrier, inc=1, device_id=device, device_id_type=MESH)

    def remote(src, dst, send_sem, recv_sem, device):
        return pltpu.make_async_remote_copy(
            src_ref=src, dst_ref=dst, send_sem=send_sem, recv_sem=recv_sem, device_id=device, device_id_type=MESH
        )

    forget_acc = jnp.zeros((2 * 64, 2 * DK), F32)
    value_acc = jnp.zeros((2 * 64, 2 * DK), F32)
    for c in range(CHUNKS):
        for copy in loads[c]:
            copy.wait()
        ks = pl.ds(c * depth, depth)
        block = tok_v[:, ks]
        forget_acc += jnp.dot(block, wf_v[ks, :], preferred_element_type=F32)
        value_acc += jnp.dot(block, wv_v[ks, :], preferred_element_type=F32)
    for copy in smalls:
        copy.wait()
    forget_pre = forget_acc.astype(BF16).astype(F32)
    values = value_acc.astype(BF16)

    def sigmoid(x):
        return 1.0 / (1.0 + jnp.exp(-x))

    key_gate = sigmoid(-floor_v[...]) * sigmoid(-forget_pre)
    log_keep = jnp.log1p(-key_gate)
    for n in range(2):
        total = jnp.sum(log_keep[64 * n : 64 * n + 64], axis=0, keepdims=True)
        for h in range(2):
            total1[2 * n + h] = total[:, DK * h : DK * (h + 1)]

    pos = lax.broadcasted_iota(jnp.int32, (128, 128), 0)
    later = lax.broadcasted_iota(jnp.int32, (128, 128), 1)
    after = jnp.where((later > pos) & (later // 64 == pos // 64), 1.0, 0.0).astype(F32)
    decay = jnp.dot(after, log_keep, preferred_element_type=F32, precision=lax.Precision.HIGHEST)
    weighted = (key_gate * jnp.exp(decay)).astype(BF16)

    key_of = 16 * ((pos % 32) // 4) + 4 * (pos // 32) + pos % 4
    permute = jnp.where(later == key_of, 1.0, 0.0).astype(BF16)
    first = lax.broadcasted_iota(jnp.int32, (128, DK), 0) < 64
    for h in range(2):
        cols = slice(DK * h, DK * (h + 1))
        keys = lax.dot_general(
            permute, weighted[:, cols], (((1,), (1,)), ((), ())), preferred_element_type=F32
        ).astype(BF16)
        v = values[:, cols].astype(F32)
        both = jnp.concatenate([jnp.where(first, v, 0.0), jnp.where(first, 0.0, v)], axis=1).astype(BF16)
        own = jnp.dot(keys, both, preferred_element_type=F32).astype(BF16)
        for n in range(2):
            send1[2 * n + h] = own[:, DK * n : DK * (n + 1)]

    pl.semaphore_wait(barrier, len(partners))

    def rows_for(other):
        return send1.at[other % 4, pl.ds(pl.multiple_of(ROWS * (other // 4), ROWS), ROWS)]

    sends = []
    for j in range(1, PLANE):
        other, device = in_plane(j)
        sends.append(remote(total1.at[other % 4], rtotal1.at[me], st1.at[j], rt1.at[me], device))
        sends[-1].start()
        sends.append(remote(rows_for(other), recv1.at[me], s1.at[j], r1.at[me], device))
        sends[-1].start()
    recv1[me] = send1[pair, pl.ds(pl.multiple_of(ROWS * slice_m, ROWS), ROWS)]
    rtotal1[me] = total1[pair]

    r = lax.broadcasted_iota(jnp.int32, (ROWS, DK), 0)
    lane = lax.broadcasted_iota(jnp.int32, (ROWS, DK), 1)
    is_key = lane == 16 * (r // 4) + 4 * slice_m + r % 4

    def column(row):
        return jnp.sum(jnp.where(is_key, row, 0.0), axis=1, keepdims=True)

    q = query_v[...].astype(F32)
    q = q * sigmoid(q)
    q_row = jnp.zeros((1, DK), F32)
    for n in range(2):
        for h in range(2):
            q_row += jnp.where(pair == 2 * n + h, q[n : n + 1, DK * h : DK * (h + 1)], 0.0)
    q_col = column(q_row)

    for j in range(1, PLANE):
        other, device = in_plane(j)
        remote(total1.at[0], rtotal1.at[other], st1.at[0], rt1.at[other], device).wait_recv()
        remote(rows_for(other), recv1.at[other], s1.at[0], r1.at[other], device).wait_recv()

    state = jnp.zeros((ROWS, DK), F32)
    total = jnp.zeros((1, DK), F32)
    for s in range(PLANE):
        row = rtotal1[s]
        state = column(jnp.exp(row)) * state + recv1[s].astype(F32)
        total = total + row
    send3[...] = state.astype(BF16)
    total3[...] = total

    for j in SENDS:
        other, device = in_line(j)
        sends.append(remote(total3, rtotal3.at[group], st3.at[j], rt3.at[group], device))
        sends[-1].start()
        sends.append(remote(send3, recv3.at[group], s3.at[j], r3.at[group], device))
        sends[-1].start()
    recv3[group] = send3[...]
    rtotal3[group] = total3[...]
    for j in SENDS[::-1]:
        other, device = in_line(j)
        remote(total3, rtotal3.at[other], st3.at[0], rt3.at[other], device).wait_recv()
        remote(send3, recv3.at[other], s3.at[0], r3.at[other], device).wait_recv()
    state = jnp.zeros((ROWS, DK), F32)
    for g in range(GROUPS):
        state = column(jnp.exp(rtotal3[g])) * state + recv3[g].astype(F32)

    part4[...] = jnp.sum(q_col * state, axis=0, keepdims=True)
    for j in range(1, PLANE):
        other, device = in_plane(j)
        sends.append(remote(part4, recv4.at[me], s4.at[j], r4.at[me], device))
        sends[-1].start()
    recv4[me] = part4[...]
    for i in range(4):
        row4[i] = jnp.sum(jnp.where(r == 4 * group + i, state, 0.0), axis=0, keepdims=True)

    def in_column(j):
        other = (pair + j) % 4
        return other, (sp - pair + other, tp)

    for j in range(1, 4):
        other, device = in_column(j)
        sends.append(remote(row4.at[other], rrow4.at[pair], sr4.at[j], rr4.at[pair], device))
        sends[-1].start()
    rrow4[pair] = row4[pair]

    g = gate_v[...].astype(F32)
    g = g * sigmoid(g)
    load_out.wait()
    for j in range(1, PLANE):
        other, device = in_plane(j)
        remote(part4, recv4.at[other], s4.at[0], r4.at[other], device).wait_recv()
    reads = []
    for p in range(4):
        n, h = p // 2, p % 2
        raw = recv4[p] + recv4[4 + p] + recv4[8 + p] + recv4[12 + p]
        scale = lax.rsqrt(jnp.mean(raw * raw, axis=-1, keepdims=True) + EPSILON)
        reads.append(raw * scale * gain_v[...] * g[n : n + 1, DK * h : DK * (h + 1)])
    row8 = lax.broadcasted_iota(jnp.int32, (8, DK), 0)
    heads = [jnp.where(row8 == 0, reads[h], jnp.where(row8 == 1, reads[2 + h], 0.0)) for h in range(2)]
    read = jnp.concatenate(heads, axis=1).astype(BF16)
    width = decode_out.shape[1]
    for t in range(N_TP):
        term = jnp.dot(read, wo_v[:, t * width : (t + 1) * width], preferred_element_type=F32)
        send5[t] = term[0:2].astype(BF16)

    for j in range(1, N_TP):
        other, device = in_tp(j)
        sends.append(remote(send5.at[other], recv5.at[tp], s5.at[j], r5.at[tp], device))
        sends[-1].start()
    recv5[tp] = send5[tp]
    for j in range(1, 4):
        other, device = in_column(j)
        remote(row4.at[0], rrow4.at[other], sr4.at[0], rr4.at[other], device).wait_recv()
    for p in range(4):
        state_out[p // 2, p % 2] = rrow4[p].astype(BF16)
    for j in range(1, N_TP):
        other, device = in_tp(j)
        remote(send5.at[0], recv5.at[other], s5.at[0], r5.at[other], device).wait_recv()
    out = recv5[0].astype(F32)
    for t in range(1, N_TP):
        out += recv5[t].astype(F32)
    decode_out[...] = out.astype(BF16)
    for copy in sends:
        copy.wait_send()


def on_device(tokens, w_forget, w_value, floor_logit, norm_gain, query_new, gate_new, w_out):
    flat = tokens.reshape(-1, tokens.shape[-1])
    any_spec = pl.BlockSpec(memory_space=pl.ANY)
    vmem_spec = pl.BlockSpec(memory_space=pltpu.VMEM)
    dma = pltpu.SemaphoreType.DMA
    return pl.pallas_call(
        kernel,
        name="final_states",
        out_shape=(
            jax.ShapeDtypeStruct((2, 2, 1, DK), BF16),
            jax.ShapeDtypeStruct((2, w_out.shape[1] // N_TP), BF16),
        ),
        in_specs=[any_spec] * 8,
        out_specs=(vmem_spec, vmem_spec),
        scratch_shapes=[
            pltpu.VMEM(flat.shape, BF16),
            pltpu.VMEM(w_forget.shape, BF16),
            pltpu.VMEM(w_value.shape, BF16),
            pltpu.VMEM(w_out.shape, BF16),
            pltpu.VMEM((1, 2 * DK), F32),
            pltpu.VMEM((1, DK), F32),
            pltpu.VMEM((2, 2 * DK), BF16),
            pltpu.VMEM((2, 2 * DK), BF16),
            pltpu.VMEM((4, DK, DK), BF16),
            pltpu.VMEM((4, 1, DK), F32),
            pltpu.VMEM((PLANE, ROWS, DK), BF16),
            pltpu.VMEM((PLANE, 1, DK), F32),
            pltpu.VMEM((ROWS, DK), BF16),
            pltpu.VMEM((1, DK), F32),
            pltpu.VMEM((GROUPS, ROWS, DK), BF16),
            pltpu.VMEM((GROUPS, 1, DK), F32),
            pltpu.VMEM((1, DK), F32),
            pltpu.VMEM((PLANE, 1, DK), F32),
            pltpu.VMEM((4, 1, DK), F32),
            pltpu.VMEM((4, 1, DK), F32),
            pltpu.VMEM((N_TP, 2, w_out.shape[1] // N_TP), BF16),
            pltpu.VMEM((N_TP, 2, w_out.shape[1] // N_TP), BF16),
            dma((3 * CHUNKS,)),
            dma((4,)),
            dma,
            dma((PLANE,)), dma((PLANE,)), dma((PLANE,)), dma((PLANE,)),
            dma((GROUPS,)), dma((GROUPS,)), dma((GROUPS,)), dma((GROUPS,)),
            dma((PLANE,)), dma((PLANE,)), dma((4,)), dma((4,)),
            dma((N_TP,)), dma((N_TP,)),
        ],
        compiler_params=pltpu.CompilerParams(collective_id=0, has_side_effects=True),
    )(flat, w_forget, w_value, floor_logit.reshape(1, -1), norm_gain.reshape(1, -1), query_new, gate_new, w_out)


def solution(mesh):
    return jax.shard_map(
        on_device,
        mesh=mesh,
        in_specs=(
            P(None, "sp", None),
            P(None, "tp"),
            P(None, "tp"),
            P("tp"),
            P(),
            P(None, "tp"),
            P(None, "tp"),
            P("tp", None),
        ),
        out_specs=(P(None, "tp", "sp", None), P(None, "tp")),
        check_vma=False,
    )
```

time: 674 us -> 60.8 us (0.09)
  waiting for transfers between devices: 290 us -> 0 us
  blocking collectives: 218 us -> 0 us
  other arithmetic: 90.9 us -> 0 us
  Pallas kernels: 0 us -> 57.5 us
  starting transfers between devices: 42.1 us -> 0 us
  between operations: 14.8 us -> 0.64 us
  matrix products: 7.32 us -> 0 us
    unnamed x2 -> x0, waiting for transfers between devices: 286 us -> none
    all_gather x1 -> x0, blocking collectives: 162 us -> none  [prefix(): pieces = lax.all_gather(value, axis)]
    select_n x127 -> x0, other arithmetic: 86.5 us -> none  [hop(): return jnp.where(position < mine, longer, running)]
    pallas_call x0 -> x1, Pallas kernels: none -> 57.5 us  [on_device(): pl.pallas_call(kernel, name='final_states', out_shape=(jax.ShapeDtypeStru...]
    psum x2 -> x0, blocking collectives: 46.8 us -> none  [over_axes(): return functools.reduce(lax.psum, axes, x)]
    all_to_all x1 -> x0, starting transfers between devices: 42.1 us -> none  [sent_and_summed(): lax.all_to_all(tiles, axis, split_axis=0, concat_axis=0, tiled=True)]
    unnamed x1 -> x0, blocking collectives: 8.79 us -> none
    dot_general x4 -> x0, matrix products: 7.32 us -> none  [the longest x1 2.57 us: on_device(): out_term = jnp.dot(read, w_out, preferred_element_type=jnp.float32)]
  transfers between devices with their start and end apart: 2 -> 0, of which waited for: 2 -> 0; matrix products, arithmetic and copies ran while one was open for 1% -> 0% of each run, Pallas kernels for 0% -> 0%
where the time goes in v1:
time: 60.8 us; the launch traced here: 60.6 us
  Pallas kernels  57.5 us (95%)
  local copies, waits for them, and re-layouts  2.47 us (4%)
  between operations  0.64 us (1%)
    pallas_call x1, Pallas kernels, on_device(): pl.pallas_call(kernel, name='final_states', out_shape=(jax.ShapeDtypeStru...  57.5 us
    pallas_call x1, local copies, waits for them, and re-layouts, on_device(): pl.pallas_call(kernel, name='final_states', out_shape=(jax.ShapeDtypeStru...  1.24 us
    unnamed x1, local copies, waits for them, and re-layouts  1.23 us

profile of v1, /device:TPU:1, one launch (start us, length us, event | category | flops | bytes accessed | tf_op | source)
XLA Modules:
  0.0 60.6 jit_solution(5113417693000351979)
XLA Ops:
  0.6 57.5 %final_states.1 = (bf16[2,2,1,128]{3,2,1,0:T(2,128)(2,1)}, bf16[2,512]{1,0:T(2,128)(2,1)}) custom-call(bf16[128,4096]{1,0:T(8,128)(2,1)} %bitcast.3, bf16[4096,256]{1,0:T(8,128)(2,1)} %w_forget.1, bf16[4096,256]{1,0:T(8,128)(2,1)} %w_value.1, f32[1,256]{1,0:T(1,128)} %bitcast.4, f32[1,128]{1,0:T(1,128)} %bitcast.5, bf16[2,256]{1,0:T(2,128)(2,1)} %query.1, ...), custom_call_target="tpu_custom_call" | custom-call | tf_op jit(solution)/shard_map/final_states/pallas_call | solution.py:255
  58.1 1.2 %copy.10 = bf16[2,2,1,128]{3,1,2,0:T(2,128)(2,1)} copy(bf16[2,2,1,128]{3,2,1,0:T(2,128)(2,1)} %get-tuple-element.2) | data formatting | bytes 2048 | tf_op jit(solution)/shard_map/final_states/pallas_call | solution.py:255
  59.4 1.2 %copy.12 = bf16[2,512]{1,0:T(2,128)(2,1)} copy(bf16[2,512]{1,0:T(2,128)(2,1)} %get-tuple-element.7) | data formatting | bytes 4096

commit v2 on v0

v2 whole, which is shorter than its diff:
```python
import functools

import jax
import jax.numpy as jnp
from jax import lax
from jax.experimental import pallas as pl
from jax.experimental.pallas import tpu as pltpu
from jax.sharding import PartitionSpec as P

MESH = pl.DeviceIdType.MESH
F32 = jnp.float32
BF16 = jnp.bfloat16
EPSILON = 1e-06

DK = 128
SPAN = 64
NY = 4
NZ = 32
N_TP = 8
CHUNKS = 4
TURN = 17
ORDER = sorted(range(1, NZ), key=lambda z: 11 + 1.55 * z if z < TURN else 30 + 0.6 * (NZ - z))


def kernel(
    tok, w_forget, w_value, floor, gain, query, gate, w_out,
    state_out, decode_out,
    tok_v, wf_v, wv_v, wcols, floor_v, gain_v, query_v, gate_v,
    send1, total1, recv1, rtotal1,
    send3, total3, recv3, rtotal3,
    read4, recv4, final, block, row5, rrow5, decode,
    in_sem, small_sem, w_own, w_send, w_recv,
    s1, r1, st1, rt1, s3, r3, st3, rt3, s4, r4, sblock, rblock, s5, r5, sdec, rdec,
):
    sp, tp = lax.axis_index("sp"), lax.axis_index("tp")
    z, pair = sp // NY, sp % NY
    depth = tok.shape[1] // CHUNKS
    width = decode.shape[1]

    loads = []
    for c in range(CHUNKS):
        ks = pl.ds(c * depth, depth)
        loads.append([
            pltpu.make_async_copy(tok.at[:, ks], tok_v.at[:, ks], in_sem.at[3 * c]),
            pltpu.make_async_copy(w_forget.at[ks], wf_v.at[ks], in_sem.at[3 * c + 1]),
            pltpu.make_async_copy(w_value.at[ks], wv_v.at[ks], in_sem.at[3 * c + 2]),
        ])
    smalls = [
        pltpu.make_async_copy(src, dst, small_sem.at[i])
        for i, (src, dst) in enumerate(((floor, floor_v), (gain, gain_v), (query, query_v), (gate, gate_v)))
    ]
    for copy in loads[0]:
        copy.start()
    for copy in smalls:
        copy.start()
    for chunk in loads[1:]:
        for copy in chunk:
            copy.start()

    barrier = pltpu.get_barrier_semaphore()

    def signal(device):
        pl.semaphore_signal(barrier, inc=1, device_id=device, device_id_type=MESH)

    def in_column(j):
        other = (pair + j) % NY
        return other, (sp - pair + other, tp)

    mine = pair * N_TP + tp

    def in_root(j):
        other = (mine + j) % (NY * N_TP)
        return other, (other // N_TP, other % N_TP)

    def in_line(other):
        return (other * NY + pair, tp)

    for j in range(1, NY):
        signal(in_column(j)[1])

    @pl.when(z == 0)
    def _():
        for other in range(1, NZ):
            signal(in_line(other))
        for j in range(1, NY * N_TP):
            if j % N_TP:
                signal(in_root(j)[1])

    def remote(src, dst, send_sem, recv_sem, device):
        return pltpu.make_async_remote_copy(
            src_ref=src, dst_ref=dst, send_sem=send_sem, recv_sem=recv_sem, device_id=device, device_id_type=MESH
        )

    forget_acc = jnp.zeros((2 * SPAN, 2 * DK), F32)
    value_acc = jnp.zeros((2 * SPAN, 2 * DK), F32)
    for c in range(CHUNKS):
        for copy in loads[c]:
            copy.wait()
        ks = pl.ds(c * depth, depth)
        part = tok_v[:, ks]
        forget_acc += jnp.dot(part, wf_v[ks, :], preferred_element_type=F32)
        value_acc += jnp.dot(part, wv_v[ks, :], preferred_element_type=F32)
    for copy in smalls:
        copy.wait()
    forget_pre = forget_acc.astype(BF16).astype(F32)
    values_t = value_acc.astype(BF16).astype(F32).T.astype(BF16)

    def sigmoid(x):
        return 1.0 / (1.0 + jnp.exp(-x))

    key_gate = sigmoid(-floor_v[...]) * sigmoid(-forget_pre)
    log_keep = jnp.log1p(-key_gate)
    for n in range(2):
        total = jnp.sum(log_keep[SPAN * n : SPAN * (n + 1)], axis=0, keepdims=True)
        for h in range(2):
            total1[2 * n + h] = total[:, DK * h : DK * (h + 1)]

    pos = lax.broadcasted_iota(jnp.int32, (128, 128), 0)
    lane = lax.broadcasted_iota(jnp.int32, (128, 128), 1)
    after = jnp.where((lane > pos) & (lane // SPAN == pos // SPAN), 1.0, 0.0).astype(F32)
    decay = jnp.dot(after, log_keep, preferred_element_type=F32, precision=lax.Precision.HIGHEST)
    weighted = key_gate * jnp.exp(decay)
    first = pos < SPAN
    for h in range(2):
        w = weighted[:, DK * h : DK * (h + 1)]
        both = jnp.concatenate([jnp.where(first, w, 0.0), jnp.where(first, 0.0, w)], axis=1).astype(BF16)
        own = jnp.dot(values_t[DK * h : DK * (h + 1)], both, preferred_element_type=F32).astype(BF16)
        for n in range(2):
            send1[2 * n + h] = own[:, DK * n : DK * (n + 1)]

    pl.semaphore_wait(barrier, jnp.where(z == 0, NY * N_TP - 1, NY))
    column = []
    for j in range(1, NY):
        other, device = in_column(j)
        column.append(remote(total1.at[other], rtotal1.at[pair], st1.at[j], rt1.at[pair], device))
        column.append(remote(send1.at[other], recv1.at[pair], s1.at[j], r1.at[pair], device))
    for copy in column:
        copy.start()
    recv1[pair] = send1[pair]
    rtotal1[pair] = total1[pair]

    def w_columns(t):
        return w_out.at[:, pl.ds(pl.multiple_of(width * t, width), width)]

    w_local = pltpu.make_async_copy(w_columns(tp), wcols.at[tp], w_own)

    def w_copy(j):
        other = (tp + j) % N_TP
        return remote(w_columns(other), wcols.at[tp], w_send.at[j], w_recv.at[tp], (sp, other))

    @pl.when(z == 0)
    def _():
        for j in range(1, N_TP):
            w_copy(j).start()
        w_local.start()

    for j in range(1, NY):
        other, device = in_column(j)
        remote(total1.at[0], rtotal1.at[other], st1.at[0], rt1.at[other], device).wait_recv()
        remote(send1.at[0], recv1.at[other], s1.at[0], r1.at[other], device).wait_recv()
    state = recv1[0].astype(F32)
    total = rtotal1[0]
    for s in range(1, NY):
        row = rtotal1[s]
        state = jnp.exp(row) * state + recv1[s].astype(F32)
        total = total + row
    send3[...] = state.astype(BF16)
    total3[...] = total

    def pass_rows():
        r8 = lax.broadcasted_iota(jnp.int32, (8, DK), 0)
        rows = block[...]
        for i in range(NY):
            row5[i] = jnp.sum(jnp.where(r8 == NY * (z % 2) + i, rows, 0.0), axis=0, keepdims=True)
        for j in range(1, NY):
            other, device = in_column(j)
            remote(row5.at[other], rrow5.at[pair], s5.at[j], r5.at[pair], device).start()
        rrow5[pair] = row5[pair]

    def wait_rows():
        for j in range(1, NY):
            other, device = in_column(j)
            remote(row5.at[0], rrow5.at[other], s5.at[0], r5.at[other], device).wait_recv()

    def state_to_root(source):
        return (
            remote(total3, rtotal3.at[source], st3, rt3.at[source], in_line(0)),
            remote(send3, recv3.at[source], s3, r3.at[source], in_line(0)),
        )

    def block_to(other):
        rows = pl.ds(8 * (other // 2), 8)
        return remote(final.at[rows], block, sblock.at[other], rblock, in_line(other))

    def decode_to(other):
        return remote(decode, decode, sdec.at[other], rdec, in_line(other))

    @pl.when(z != 0)
    def _():
        for copy in state_to_root(z):
            copy.start()
        block_to(1).wait_recv()
        pass_rows()
        wait_rows()
        decode_to(1).wait_recv()
        for copy in state_to_root(z):
            copy.wait_send()

    @pl.when(z == 0)
    def _():
        def of_pair(x):
            row = jnp.zeros((1, DK), F32)
            for p in range(NY):
                n, h = p // 2, p % 2
                row += jnp.where(pair == p, x[n : n + 1, DK * h : DK * (h + 1)], 0.0)
            return row * sigmoid(row)

        q_row = of_pair(query_v[...].astype(F32))
        out_gate = gain_v[...] * of_pair(gate_v[...].astype(F32))
        lower = send3[...].astype(F32)
        upper = jnp.zeros((DK, DK), F32)
        upper_keep = jnp.ones((1, DK), F32)
        for i, source in enumerate(ORDER):
            if i == 20:
                pass
            for copy in state_to_root(source):
                copy.wait_recv()
            keep = jnp.exp(rtotal3[source])
            incoming = recv3[source].astype(F32)
            if source < TURN:
                lower = keep * lower + incoming
            else:
                upper = upper + upper_keep * incoming
                upper_keep = upper_keep * keep
        state_t = upper + upper_keep * lower

        raw = jnp.sum(q_row * state_t, axis=1, keepdims=True)
        scale = lax.rsqrt(jnp.mean(raw * raw, axis=0, keepdims=True) + EPSILON)
        raw_row = jnp.sum(jnp.where(pos == lane, raw, 0.0), axis=0, keepdims=True)
        read4[...] = raw_row * scale * out_gate
        for j in range(1, NY * N_TP):
            other, device = in_root(j)
            remote(read4, recv4.at[mine], s4.at[j], r4.at[mine], device).start()
        recv4[mine] = read4[...]

        rows = state_t.T
        final[...] = rows
        block[...] = rows[0:8]
        for other in range(1, NZ):
            block_to(other).start()
        pass_rows()
        for j in range(1, N_TP):
            other = (tp + j) % N_TP
            remote(w_columns(0), wcols.at[other], w_send.at[0], w_recv.at[other], (sp, other)).wait_recv()
        w_local.wait()

        for j in range(1, NY * N_TP):
            other, device = in_root(j)
            remote(read4, recv4.at[other], s4.at[0], r4.at[other], device).wait_recv()
        r8 = lax.broadcasted_iota(jnp.int32, (8, DK), 0)
        out = jnp.zeros((8, width), F32)
        for t in range(N_TP):
            heads = [
                jnp.where(r8 == 0, recv4[h * N_TP + t], jnp.where(r8 == 1, recv4[(2 + h) * N_TP + t], 0.0))
                for h in range(2)
            ]
            read = jnp.concatenate(heads, axis=1).astype(BF16)
            out += jnp.dot(read, wcols[t], preferred_element_type=F32).astype(BF16).astype(F32)
        decode[...] = out[0:2].astype(BF16)
        for other in range(1, NZ):
            decode_to(other).start()
        wait_rows()
        for j in range(1, N_TP):
            w_copy(j).wait_send()
        for j in range(1, NY * N_TP):
            remote(read4, recv4.at[mine], s4.at[j], r4.at[mine], in_root(j)[1]).wait_send()
        for other in range(1, NZ):
            block_to(other).wait_send()
        for other in range(1, NZ):
            decode_to(other).wait_send()

    for copy in column:
        copy.wait_send()
    for j in range(1, NY):
        remote(row5.at[0], rrow5.at[pair], s5.at[j], r5.at[pair], in_column(j)[1]).wait_send()
    for p in range(NY):
        n, h = p // 2, p % 2
        state_out[n, h : h + 1] = rrow5[p].astype(BF16)
    decode_out[...] = decode[...]


def on_device(tokens, w_forget, w_value, floor_logit, norm_gain, query_new, gate_new, w_out):
    flat = tokens.reshape(-1, tokens.shape[-1])
    width = w_out.shape[1] // N_TP
    any_spec = pl.BlockSpec(memory_space=pl.ANY)
    vmem_spec = pl.BlockSpec(memory_space=pltpu.VMEM)
    dma = pltpu.SemaphoreType.DMA
    state, decode = pl.pallas_call(
        kernel,
        name="final_states",
        out_shape=(pltpu.VMEM((2, 2, DK), BF16), pltpu.VMEM((2, width), BF16)),
        in_specs=[any_spec] * 8,
        out_specs=(vmem_spec, vmem_spec),
        scratch_shapes=[
            pltpu.VMEM(flat.shape, BF16),
            pltpu.VMEM(w_forget.shape, BF16),
            pltpu.VMEM(w_value.shape, BF16),
            pltpu.VMEM((N_TP, w_out.shape[0], width), BF16),
            pltpu.VMEM((1, 2 * DK), F32),
            pltpu.VMEM((1, DK), F32),
            pltpu.VMEM((2, 2 * DK), BF16),
            pltpu.VMEM((2, 2 * DK), BF16),
            pltpu.VMEM((NY, DK, DK), BF16),
            pltpu.VMEM((NY, 1, DK), F32),
            pltpu.VMEM((NY, DK, DK), BF16),
            pltpu.VMEM((NY, 1, DK), F32),
            pltpu.VMEM((DK, DK), BF16),
            pltpu.VMEM((1, DK), F32),
            pltpu.VMEM((NZ, DK, DK), BF16),
            pltpu.VMEM((NZ, 1, DK), F32),
            pltpu.VMEM((1, DK), F32),
            pltpu.VMEM((NY * N_TP, 1, DK), F32),
            pltpu.VMEM((DK, DK), F32),
            pltpu.VMEM((8, DK), F32),
            pltpu.VMEM((NY, 1, DK), F32),
            pltpu.VMEM((NY, 1, DK), F32),
            pltpu.VMEM((2, width), BF16),
            dma((3 * CHUNKS,)), dma((4,)), dma, dma((N_TP,)), dma((N_TP,)),
            dma((NY,)), dma((NY,)), dma((NY,)), dma((NY,)),
            dma, dma((NZ,)), dma, dma((NZ,)),
            dma((NY * N_TP,)), dma((NY * N_TP,)),
            dma((NZ,)), dma, dma((NY,)), dma((NY,)), dma((NZ,)), dma,
        ],
        compiler_params=pltpu.CompilerParams(collective_id=0, has_side_effects=True),
    )(flat, w_forget, w_value, floor_logit.reshape(1, -1), norm_gain.reshape(1, -1), query_new, gate_new, w_out)
    return state.reshape(2, 2, 1, DK), decode


def solution(mesh):
    return jax.shard_map(
        on_device,
        mesh=mesh,
        in_specs=(
            P(None, "sp", None),
            P(None, "tp"),
            P(None, "tp"),
            P("tp"),
            P(),
            P(None, "tp"),
            P(None, "tp"),
            P("tp", None),
        ),
        out_specs=(P(None, "tp", "sp", None), P(None, "tp")),
        check_vma=False,
    )
```

time: 674 us -> 50.6 us (0.08)
  waiting for transfers between devices: 290 us -> 0 us
  blocking collectives: 218 us -> 0 us
  other arithmetic: 90.9 us -> 0 us
  Pallas kernels: 0 us -> 48.7 us
  starting transfers between devices: 42.1 us -> 0 us
  between operations: 14.8 us -> 0.64 us
  matrix products: 7.32 us -> 0 us
    unnamed x2 -> x0, waiting for transfers between devices: 286 us -> none
    all_gather x1 -> x0, blocking collectives: 162 us -> none  [prefix(): pieces = lax.all_gather(value, axis)]
    select_n x127 -> x0, other arithmetic: 86.5 us -> none  [hop(): return jnp.where(position < mine, longer, running)]
    pallas_call x0 -> x1, Pallas kernels: none -> 48.7 us  [on_device(): pl.pallas_call(kernel, name='final_states', out_shape=(pltpu.VMEM((2, 2,...]
    psum x2 -> x0, blocking collectives: 46.8 us -> none  [over_axes(): return functools.reduce(lax.psum, axes, x)]
    all_to_all x1 -> x0, starting transfers between devices: 42.1 us -> none  [sent_and_summed(): lax.all_to_all(tiles, axis, split_axis=0, concat_axis=0, tiled=True)]
    unnamed x1 -> x0, blocking collectives: 8.79 us -> none
    dot_general x4 -> x0, matrix products: 7.32 us -> none  [the longest x1 2.57 us: on_device(): out_term = jnp.dot(read, w_out, preferred_element_type=jnp.float32)]
  transfers between devices with their start and end apart: 2 -> 0, of which waited for: 2 -> 0; matrix products, arithmetic and copies ran while one was open for 1% -> 0% of each run, Pallas kernels for 0% -> 0%
where the time goes in v2:
time: 50.6 us; the launch traced here: 50.5 us
  Pallas kernels  48.7 us (96%)
  local copies, waits for them, and re-layouts  1.14 us (2%)
  between operations  0.64 us (1%)
    pallas_call x1, Pallas kernels, on_device(): pl.pallas_call(kernel, name='final_states', out_shape=(pltpu.VMEM((2, 2,...  48.7 us
    unnamed x2, local copies, waits for them, and re-layouts  1.14 us

profile of v2, /device:TPU:1, one launch (start us, length us, event | category | flops | bytes accessed | tf_op | source)
XLA Modules:
  0.0 50.5 jit_solution(8598212688022211255)
XLA Ops:
  0.6 48.7 %final_states.1 = (bf16[2,2,128]{2,1,0:T(2,128)(2,1)S(1)}, bf16[2,512]{1,0:T(2,128)(2,1)S(1)}) custom-call(bf16[128,4096]{1,0:T(8,128)(2,1)} %bitcast.7, bf16[4096,256]{1,0:T(8,128)(2,1)} %w_forget.1, bf16[4096,256]{1,0:T(8,128)(2,1)} %w_value.1, f32[1,256]{1,0:T(1,128)} %bitcast.8, f32[1,128]{1,0:T(1,128)} %bitcast.9, bf16[2,256]{1,0:T(2,128)(2,1)} %query.1, ...), custom_call_target="tpu_custom_call" | custom-call | tf_op jit(solution)/shard_map/final_states/pallas_call | solution.py:298
  49.3 0.6 %copy.13 = bf16[2,2,1,128]{3,1,2,0:T(2,128)(2,1)} copy(bf16[2,2,1,128]{3,1,2,0:T(2,128)(2,1)S(1)} %bitcast.6) | data formatting | bytes 2048
  49.9 0.6 %copy.14 = bf16[2,512]{1,0:T(2,128)(2,1)} copy(bf16[2,512]{1,0:T(2,128)(2,1)S(1)} %get-tuple-element.9) | data formatting | bytes 4096
